TPU v7x, 256 devices: a 8x8x2 block of a 8x8x16 slice. The times are simulated.
256 devices in a mesh: grp: 2 (over z), ep: 64 (over y, x), tp: 2 (over core).
Axes of the slice: x: 8, y: 8, z: 2, core: 2. Of those that a mesh axis runs over, the one named last changes fastest.
The devices are a block of a 8x8x16 slice.
Arguments:
- hidden_in: bfloat16 [2048, 2048], P(('grp', 'ep', 'tp')), parts along dimension 0, may hold values from -6 to 6
- query_nope: bfloat16 [2048, 16, 64], P(('grp', 'ep', 'tp')), parts along dimension 0, may hold values from -102 to 102
- query_rope: bfloat16 [2048, 16, 32], P(('grp', 'ep', 'tp')), parts along dimension 0, may hold values from -6 to 6
- new_latent: bfloat16 [2048, 256], P(('grp', 'ep', 'tp')), parts along dimension 0, may hold values from -6 to 6
- new_rope: bfloat16 [2048, 32], P(('grp', 'ep', 'tp')), parts along dimension 0, may hold values from -6 to 6
- cache_latent: bfloat16 [2048, 1024, 256], P(('grp', 'ep', 'tp')), parts along dimension 0, may hold values from -6 to 6
- cache_rope: bfloat16 [2048, 1024, 32], P(('grp', 'ep', 'tp')), parts along dimension 0, may hold values from -6 to 6
- lengths: int32 [2048], P(('grp', 'ep', 'tp')), parts along dimension 0, may hold values from 1 to 1024, as said below
- absorb_key: bfloat16 [256, 16, 64], replicated, may hold values from -0.75 to 0.75
- value_up: bfloat16 [256, 16, 128], replicated, may hold values from -0.375 to 0.375
- out_proj: bfloat16 [2048, 2048], P(None, ('ep', 'tp')), may hold values from -0.125 to 0.125
- gain_mix: bfloat16 [2048], replicated, may hold values from 0.099609375 to 1.8984375
- gain_ffn_in: bfloat16 [2048], replicated, may hold values from 0.099609375 to 1.8984375
- router: bfloat16 [2048, 128], replicated, may hold values from -0.125 to 0.125
- routes: int32 [2048, 6], P(('grp', 'ep')), parts along dimension 0, may hold values from 0 to 127, all different within a row; in each aligned block of 16 rows (0 to 15, 16 to 31, ...) at most 2 rows name the same one
- expert_gate: bfloat16 [128, 2048, 256], P(('ep', 'tp')), may hold values from -0.125 to 0.125
- expert_up: bfloat16 [128, 2048, 256], P(('ep', 'tp')), may hold values from -0.125 to 0.125
- expert_down: bfloat16 [128, 256, 2048], P(('ep', 'tp')), may hold values from -0.375 to 0.375
- shared_gate: bfloat16 [2048, 256], replicated, may hold values from -0.125 to 0.125
- shared_up: bfloat16 [2048, 256], replicated, may hold values from -0.125 to 0.125
- shared_down: bfloat16 [256, 2048], replicated, may hold values from -0.375 to 0.375
- gain_ffn_out: bfloat16 [2048], replicated, may hold values from 0.099609375 to 1.8984375
Outputs:
- layer_out: bfloat16 [2048, 2048], P(('grp', 'ep', 'tp')), parts along dimension 0
There are 2 independent parts, one for each index of `grp`. A program takes and returns all parts, laid end to end along the dimension named above; an argument that names none is the same for every part. Nothing has to cross between parts.
Inputs may be any that keep to these rules, and one draw needn't show every extreme that they name: `lengths`: every sequence holds 1 to 1024 cached positions, and some sequence holds 1024. `routes`: each row names 6 different experts; in each aligned block of 16 rows (the rows of one index of ep) no expert is named by more than 2 rows, and in some block some expert is named by exactly 2 rows.
All inputs are finite; a program needn't handle non-finite values.
Results may differ from a plain program's by a relative error of at most 0.015.
Values may be sent and summed in bfloat16 or wider, within the bound.
No kernel may reach another device: no remote copies, remote signals or barrier semaphores. Data moves between devices by JAX's collectives and lax.ppermute only.
A program may use at most 64 MiB of HBM per device.

v0:
```python
import math

import jax
import jax.numpy as jnp
from jax import lax
from jax.experimental import pallas as pl
from jax.experimental.pallas import tpu as pltpu
from jax.sharding import Mesh
from jax.sharding import PartitionSpec as P

SEQ_STEP = 4
OUT_CHUNKS = 4
EP = ("ep_0", "ep_1")
GRP_EP_TP = ("grp", "ep_0", "ep_1", "tp")
EP_TP = ("ep_0", "ep_1", "tp")
GRP_EP = ("grp", "ep_0", "ep_1")


rope_theta = 10000.0
norm_eps = 1e-06
routed_scale = 2.5
masked_score = -1e30


def device_at(row, col, core):
    return (row * 8 + col) * 2 + core


COLUMN_GROUPS = [
    [device_at(row, col, core) for col in range(8)] for row in range(8) for core in range(2)
]
BLOCKS = [
    [device_at(row, 2 * pair + col, core) for row in range(8) for col in range(2)]
    for pair in range(4)
    for core in range(2)
]
HALVES = 2


def repeat_kernel(array_ref, out_ref):
    run = out_ref.shape[-1]
    count = array_ref.shape[-1] // run
    for n in range(out_ref.shape[0]):
        out_ref[n] = array_ref[:, n % count * run : (n % count + 1) * run]


def in_parts(array, count, times):
    rows, width = array.shape
    return pl.pallas_call(
        repeat_kernel,
        in_specs=[pl.BlockSpec(memory_space=pltpu.VMEM)],
        out_specs=pl.BlockSpec(memory_space=pltpu.VMEM),
        out_shape=jax.ShapeDtypeStruct((count * times, rows, width // count), array.dtype),
        compiler_params=pltpu.CompilerParams(vmem_limit_bytes=4 << 20),
        name="parts",
    )(array)


def project_kernel(place_ref, heads_ref, own_slab_ref, other_slab_ref, out_ref):
    core = place_ref[0]
    heads = heads_ref[...].reshape(-1, heads_ref.shape[-1])
    dims = (((1,), (1,)), ((), ()))
    own = lax.dot_general(heads, own_slab_ref[...], dims, preferred_element_type=jnp.float32)
    other = lax.dot_general(heads, other_slab_ref[...], dims, preferred_element_type=jnp.float32)
    joined = jnp.concatenate(
        [jnp.where(core == 0, own, other), jnp.where(core == 0, other, own)], axis=-1
    ).astype(jnp.bfloat16)
    count = joined.shape[-1]
    source = lax.broadcasted_iota(jnp.int32, (count, count), 0)
    target = lax.broadcasted_iota(jnp.int32, (count, count), 1)
    run = count // 16
    goes_to = source % (count // 2) // run * (2 * run) + source // (count // 2) * run + source % run
    order = jnp.where(goes_to == target, 1.0, 0.0).astype(jnp.bfloat16)
    out = jnp.dot(joined, order, preferred_element_type=jnp.float32)
    out_ref[...] = out.astype(jnp.bfloat16).reshape(out_ref.shape)


def projected(place, heads, own_slab, other_slab):
    return pl.pallas_call(
        project_kernel,
        in_specs=[pl.BlockSpec(memory_space=pltpu.SMEM)]
        + [pl.BlockSpec(memory_space=pltpu.VMEM)] * 3,
        out_specs=pl.BlockSpec(memory_space=pltpu.VMEM),
        out_shape=jax.ShapeDtypeStruct((*heads.shape[:2], 2 * own_slab.shape[0]), jnp.bfloat16),
        compiler_params=pltpu.CompilerParams(vmem_limit_bytes=6 << 20),
        name="projected",
    )(place, heads, own_slab, other_slab)


def exchanged(blocks, groups):
    return lax.all_to_all(blocks, EP_TP, 0, 0, axis_index_groups=groups, tiled=True)


def from_other_core(array):
    return lax.ppermute(array, "tp", [(0, 1), (1, 0)])


def normalize(values):
    return values * lax.rsqrt(jnp.mean(values * values, axis=-1, keepdims=True) + norm_eps)


def attention_kernel(
    lengths_ref,
    nope_ref,
    rope_ref,
    latent_ref,
    key_ref,
    absorb_ref,
    cache_hbm,
    cache_rope_hbm,
    out_ref,
    cache_ref,
    cache_rope_ref,
    arrived,
):
    moves = []
    for n in range(cache_ref.shape[0] // SEQ_STEP):
        group = pl.ds(n * SEQ_STEP, SEQ_STEP)
        moves.append(
            (
                pltpu.make_async_copy(cache_hbm.at[group], cache_ref.at[group], arrived.at[n, 0]),
                pltpu.make_async_copy(
                    cache_rope_hbm.at[group], cache_rope_ref.at[group], arrived.at[n, 1]
                ),
            )
        )
    for pair in moves:
        for move in pair:
            move.start()
    seq_count, heads, nope = nope_ref.shape
    rope = rope_ref.shape[-1]
    half = rope // 2
    latent = cache_ref.shape[-1]
    scale = (nope + rope) ** (-0.5)

    def turned(values, cosine, sine):
        swapped = jnp.concatenate([values[..., half:], values[..., :half]], axis=-1)
        return values * cosine + swapped * sine

    rows = nope_ref[...].reshape(seq_count * heads, nope)
    twice = jnp.concatenate([rows, rows], axis=-1)
    wide = jnp.concatenate([twice] * (heads // 2), axis=-1)
    row_head = lax.broadcasted_iota(jnp.int32, wide.shape, 0) % heads
    column_head = lax.broadcasted_iota(jnp.int32, wide.shape, 1) // nope
    wide = jnp.where(row_head == column_head, wide.astype(jnp.float32), 0.0)
    queries = jnp.dot(
        wide.astype(jnp.bfloat16), absorb_ref[...], preferred_element_type=jnp.float32
    )
    query_all = queries.reshape(seq_count, heads, latent).astype(jnp.bfloat16)
    row = lax.broadcasted_iota(jnp.int32, (seq_count, rope), 0)
    column = lax.broadcasted_iota(jnp.int32, (seq_count, rope), 1)
    position = jnp.zeros((seq_count, rope), jnp.int32)
    for n in range(seq_count):
        position = jnp.where(row == n, lengths_ref[n], position)
    exponent = (column % half).astype(jnp.float32) * (-2.0 / rope * math.log(rope_theta))
    angles = position.astype(jnp.float32) * jnp.exp(exponent)
    cosine = jnp.cos(angles)
    sine = jnp.sin(angles)
    sine = jnp.where(column < half, -sine, sine)
    query_pe_all = turned(
        rope_ref[...].astype(jnp.float32), cosine[:, None, :], sine[:, None, :]
    ).astype(jnp.bfloat16)
    latent_new = normalize(latent_ref[...].astype(jnp.float32)).astype(jnp.bfloat16)
    latent_new_all = latent_new.astype(jnp.float32)[:, None, :]
    key_new = turned(key_ref[...].astype(jnp.float32), cosine, sine)
    key_new_all = key_new.astype(jnp.bfloat16).astype(jnp.float32)[:, None, :]

    for step in range(len(moves)):
        places = range(SEQ_STEP)
        seqs = [step * SEQ_STEP + place for place in places]
        rows = SEQ_STEP * heads
        group = slice(step * SEQ_STEP, (step + 1) * SEQ_STEP)
        query = query_all[group]
        query_pe = query_pe_all[group]
        latent_wide = latent_new_all[group]
        key_wide = key_new_all[group]
        for move in moves[step]:
            move.wait()
        score_new = (
            jnp.sum(query.astype(jnp.float32) * latent_wide, axis=-1, keepdims=True)
            + jnp.sum(query_pe.astype(jnp.float32) * key_wide, axis=-1, keepdims=True)
        ).reshape(rows, 1) * scale
        parts = [
            lax.dot_general(
                query[place], cache_ref[seqs[place]], (((1,), (1,)), ((), ())),
                preferred_element_type=jnp.float32,
            )
            + jnp.dot(query_pe[place], cache_rope_ref[seqs[place]], preferred_element_type=jnp.float32)
            for place in places
        ]
        position = lax.broadcasted_iota(jnp.int32, parts[0].shape, 1)
        scores = jnp.concatenate(
            [
                jnp.where(position < lengths_ref[seq], part * scale, masked_score)
                for seq, part in zip(seqs, parts)
            ],
            axis=0,
        )
        row_max = jnp.maximum(jnp.max(scores, axis=-1, keepdims=True), score_new)
        weights = jnp.exp(scores - row_max)
        weight_new = jnp.exp(score_new - row_max)
        total = jnp.sum(weights, axis=-1, keepdims=True) + weight_new
        rounded = weights.astype(jnp.bfloat16)
        summed = jnp.concatenate(
            [
                jnp.dot(
                    rounded[place * heads : (place + 1) * heads],
                    cache_ref[seqs[place]],
                    preferred_element_type=jnp.float32,
                )
                for place in places
            ],
            axis=0,
        )
        fresh = jnp.broadcast_to(latent_wide, query.shape).reshape(rows, latent)
        summed = summed + weight_new.astype(jnp.bfloat16).astype(jnp.float32) * fresh
        out_ref[group] = (summed / total).astype(jnp.bfloat16).reshape(SEQ_STEP, heads, latent)


def attended(query_nope, query_rope, new_latent, new_rope, cache_latent, cache_rope, lengths, absorb_key):
    seq_count, heads, nope = query_nope.shape
    rope = query_rope.shape[-1]
    latent = cache_latent.shape[-1]
    context = cache_latent.shape[1]
    absorb = absorb_key.transpose(1, 2, 0).reshape(heads * nope, latent)
    rope_turned = cache_rope.transpose(0, 2, 1)
    return pl.pallas_call(
        attention_kernel,
        in_specs=[pl.BlockSpec(memory_space=pltpu.SMEM)]
        + [pl.BlockSpec(memory_space=pltpu.VMEM)] * 5
        + [pl.BlockSpec(memory_space=pltpu.HBM)] * 2,
        out_specs=pl.BlockSpec(memory_space=pltpu.VMEM),
        scratch_shapes=[
            pltpu.VMEM(cache_latent.shape, jnp.bfloat16),
            pltpu.VMEM(rope_turned.shape, jnp.bfloat16),
            pltpu.SemaphoreType.DMA((seq_count // SEQ_STEP, 2)),
        ],
        out_shape=jax.ShapeDtypeStruct((seq_count, heads, latent), jnp.bfloat16),
        compiler_params=pltpu.CompilerParams(vmem_limit_bytes=60 * 1024 * 1024),
        cost_estimate=pl.CostEstimate(
            flops=8 * seq_count * heads * context * latent,
            bytes_accessed=2 * seq_count * context * (latent + rope),
            transcendentals=seq_count * heads * context,
        ),
        name="attended",
    )(
        lengths, query_nope, query_rope, new_latent, new_rope, absorb, cache_latent, rope_turned
    )


def attention(
    query_nope,
    query_rope,
    new_latent,
    new_rope,
    cache_latent,
    cache_rope,
    lengths,
    absorb_key,
    value_up,
):
    latent_out = attended(
        query_nope, query_rope, new_latent, new_rope, cache_latent, cache_rope, lengths, absorb_key
    )
    return (
        jnp.einsum("shc,chv->shv", latent_out, value_up, preferred_element_type=jnp.float32)
        .astype(jnp.bfloat16)
        .reshape(latent_out.shape[0], -1)
    )


def spread_kernel(
    place_ref,
    own_pieces_ref,
    other_pieces_ref,
    own_hidden_ref,
    other_hidden_ref,
    gain_mix_ref,
    gain_in_ref,
    routes_ref,
    outgoing_ref,
    ffn_ref,
    mix_ref,
    taken_ref,
):
    core = place_ref[0]
    half = own_hidden_ref.shape[0]
    rows = 2 * half

    def in_columns(pieces_ref):
        parts = [
            pieces_ref[HALVES * n].astype(jnp.float32) + pieces_ref[HALVES * n + 1].astype(jnp.float32)
            for n in range(pieces_ref.shape[0] // HALVES)
        ]
        return jnp.concatenate(parts, axis=-1)

    own_mixed = in_columns(own_pieces_ref)
    other_mixed = in_columns(other_pieces_ref)
    mixed = jnp.concatenate(
        [
            jnp.where(core == 0, own_mixed, other_mixed),
            jnp.where(core == 0, other_mixed, own_mixed),
        ],
        axis=0,
    )
    mixed = mixed.astype(jnp.bfloat16).astype(jnp.float32)
    own_hidden = own_hidden_ref[...].astype(jnp.float32)
    other_hidden = other_hidden_ref[...].astype(jnp.float32)
    hidden = jnp.concatenate(
        [
            jnp.where(core == 0, own_hidden, other_hidden),
            jnp.where(core == 0, other_hidden, own_hidden),
        ],
        axis=0,
    )
    after_mix = (
        hidden
        + gain_mix_ref[...].astype(jnp.float32)[None] * normalize(mixed)
    ).astype(jnp.bfloat16)
    after_wide = after_mix.astype(jnp.float32)
    ffn_in = (normalize(after_wide) * gain_in_ref[...].astype(jnp.float32)[None]).astype(jnp.bfloat16)
    ffn_ref[...] = ffn_in
    mix_ref[...] = jnp.where(core == 0, after_wide[:half], after_wide[half:]).astype(jnp.bfloat16)
    slots = taken_ref.shape[0]
    slot = lax.broadcasted_iota(jnp.int32, (slots, rows), 0)
    expert = slot // 2 * 2 + core
    named = jnp.zeros((slots, rows), jnp.float32)
    for n in range(routes_ref.shape[0]):
        named = jnp.where(routes_ref[n : n + 1, :] == expert, 1.0, named)
    earlier = jnp.where(
        lax.broadcasted_iota(jnp.int32, (rows, rows), 0)
        < lax.broadcasted_iota(jnp.int32, (rows, rows), 1),
        1.0,
        0.0,
    ).astype(jnp.bfloat16)
    before = jnp.dot(named.astype(jnp.bfloat16), earlier, preferred_element_type=jnp.float32)
    taken = jnp.where(before == (slot % 2).astype(jnp.float32), named, 0.0).astype(jnp.bfloat16)
    taken_ref[...] = taken
    outgoing = jnp.dot(taken, ffn_in, preferred_element_type=jnp.float32).astype(jnp.bfloat16)
    outgoing_ref[...] = outgoing.reshape(outgoing_ref.shape)


def spread(place, own_pieces, other_pieces, own_hidden, other_hidden, gain_mix, gain_in, routes, slots):
    rows, width = 2 * own_hidden.shape[0], own_hidden.shape[1]
    return pl.pallas_call(
        spread_kernel,
        in_specs=[pl.BlockSpec(memory_space=pltpu.SMEM)]
        + [pl.BlockSpec(memory_space=pltpu.VMEM)] * 7,
        out_specs=[pl.BlockSpec(memory_space=pltpu.VMEM)] * 4,
        out_shape=[
            jax.ShapeDtypeStruct((slots // 2, 2, width), jnp.bfloat16),
            jax.ShapeDtypeStruct((rows, width), jnp.bfloat16),
            jax.ShapeDtypeStruct((rows // 2, width), jnp.bfloat16),
            jax.ShapeDtypeStruct((slots, rows), jnp.bfloat16),
        ],
        compiler_params=pltpu.CompilerParams(vmem_limit_bytes=8 << 20),
        name="spread",
    )(
        place,
        own_pieces,
        other_pieces,
        own_hidden,
        other_hidden,
        gain_mix,
        gain_in,
        routes.T,
    )


def experts_kernel(rows_ref, gate_ref, up_ref, down_ref, out_ref):
    rows = rows_ref[...].reshape(-1, rows_ref.shape[-1])
    gate_part = jnp.dot(rows, gate_ref[...], preferred_element_type=jnp.float32)
    up_part = jnp.dot(rows, up_ref[...], preferred_element_type=jnp.float32)
    inner = (gate_part / (1.0 + jnp.exp(-gate_part)) * up_part).astype(jnp.bfloat16)
    out = jnp.dot(inner, down_ref[...], preferred_element_type=jnp.float32)
    out_ref[...] = out.astype(out_ref.dtype).reshape(out_ref.shape)


def expert_rows(rows, gate_w, up_w, down_w):
    return pl.pallas_call(
        experts_kernel,
        in_specs=[pl.BlockSpec(memory_space=pltpu.VMEM)] * 4,
        out_specs=pl.BlockSpec(memory_space=pltpu.VMEM),
        out_shape=jax.ShapeDtypeStruct(rows.shape, jnp.bfloat16),
        compiler_params=pltpu.CompilerParams(vmem_limit_bytes=10 << 20),
    )(rows, gate_w, up_w, down_w)


def gathered_kernel(place_ref, weights_ref, returned_ref, shared_ref, kept_ref, given_ref):
    core = place_ref[0]
    rows = weights_ref.shape[0] // 2
    half = rows // 2
    returned = returned_ref[...].reshape(-1, returned_ref.shape[-1])
    both = jnp.dot(weights_ref[...], returned, preferred_element_type=jnp.float32)
    routed = both[:rows] + both[rows:]
    first, second = routed[:half], routed[half:]
    shared = shared_ref[...].astype(jnp.float32)
    kept_ref[...] = jnp.where(core == 0, first, second) + shared
    given_ref[...] = jnp.where(core == 0, second, first)


def gathered(place, weights, returned, shared):
    shape = jax.ShapeDtypeStruct(shared.shape, jnp.float32)
    return pl.pallas_call(
        gathered_kernel,
        in_specs=[pl.BlockSpec(memory_space=pltpu.SMEM)]
        + [pl.BlockSpec(memory_space=pltpu.VMEM)] * 3,
        out_specs=[pl.BlockSpec(memory_space=pltpu.VMEM)] * 2,
        out_shape=[shape, shape],
        compiler_params=pltpu.CompilerParams(vmem_limit_bytes=8 << 20),
        name="gathered",
    )(place, weights, returned, shared)


def routed_kernel(
    rows_hbm,
    gate_hbm,
    up_hbm,
    down_hbm,
    out_hbm,
    rows_ref,
    gate_ref,
    up_ref,
    down_ref,
    out_ref,
    arrived,
    left,
):
    moves = [
        pltpu.make_async_copy(source, target, arrived.at[n])
        for n, (source, target) in enumerate(
            (
                (rows_hbm, rows_ref),
                (gate_hbm, gate_ref),
                (up_hbm, up_ref),
                (down_hbm, down_ref),
            )
        )
    ]
    for move in moves:
        move.start()
    moves[0].wait()
    rows = rows_ref[...].reshape(-1, rows_ref.shape[-1])
    moves[1].wait()
    gate_part = jnp.dot(rows, gate_ref[...], preferred_element_type=jnp.float32)
    moves[2].wait()
    up_part = jnp.dot(rows, up_ref[...], preferred_element_type=jnp.float32)
    inner = (gate_part / (1.0 + jnp.exp(-gate_part)) * up_part).astype(jnp.bfloat16)
    moves[3].wait()
    chunk = out_ref.shape[-1] // OUT_CHUNKS
    sent = []
    for n in range(OUT_CHUNKS):
        columns = pl.ds(n * chunk, chunk)
        out = jnp.dot(inner, down_ref[:, columns], preferred_element_type=jnp.float32)
        out_ref[:, :, columns] = out.astype(out_ref.dtype).reshape(*out_ref.shape[:2], chunk)
        sent.append(
            pltpu.make_async_copy(
                out_ref.at[:, :, columns], out_hbm.at[:, :, columns], left.at[n]
            )
        )
        sent[-1].start()
    for move in sent:
        move.wait()


def routed_rows(rows, gate_w, up_w, down_w):
    return pl.pallas_call(
        routed_kernel,
        in_specs=[pl.BlockSpec(memory_space=pltpu.HBM)] * 4,
        out_specs=pl.BlockSpec(memory_space=pltpu.HBM),
        out_shape=jax.ShapeDtypeStruct(rows.shape, jnp.bfloat16),
        scratch_shapes=[pltpu.VMEM(w.shape, w.dtype) for w in (rows, gate_w, up_w, down_w, rows)]
        + [pltpu.SemaphoreType.DMA((4,)), pltpu.SemaphoreType.DMA((OUT_CHUNKS,))],
        compiler_params=pltpu.CompilerParams(vmem_limit_bytes=64300 << 10),
        name="routed",
    )(rows, gate_w, up_w, down_w)


def local(
    hidden_in,
    query_nope,
    query_rope,
    new_latent,
    new_rope,
    cache_latent,
    cache_rope,
    lengths,
    absorb_key,
    value_up,
    out_proj,
    gain_mix,
    gain_ffn_in,
    router,
    routes,
    expert_gate,
    expert_up,
    expert_down,
    shared_gate,
    shared_up,
    shared_down,
    gain_ffn_out,
):
    seq_count, _ = hidden_in.shape
    core = lax.axis_index("tp")
    own_start = core * seq_count
    place = core[None].astype(jnp.int32)
    halves = in_parts(out_proj.T, HALVES, len(COLUMN_GROUPS[0]) // HALVES)
    slab = exchanged(halves, COLUMN_GROUPS).reshape(-1, halves.shape[-1])
    other_slab = from_other_core(slab)
    other_hidden = from_other_core(hidden_in)
    heads_out = attention(
        query_nope,
        query_rope,
        new_latent,
        new_rope,
        cache_latent,
        cache_rope,
        lengths,
        absorb_key,
        value_up,
    )
    block_heads = exchanged(in_parts(heads_out, HALVES, len(BLOCKS[0]) // HALVES), BLOCKS)
    block_heads, other_hidden = lax.optimization_barrier((block_heads, other_hidden))
    partial = projected(place, block_heads, slab, other_slab)
    pieces = exchanged(partial, BLOCKS)
    other_pieces = from_other_core(pieces)
    experts_total = router.shape[1]
    group_rows, top_count = routes.shape
    ep_count = lax.axis_size(EP)
    capacity = 2 * ((group_rows * top_count + experts_total - 1) // experts_total)
    slots = ep_count * capacity
    slot_expert = lax.iota(jnp.int32, slots) // capacity * 2 + core
    outgoing, ffn_in, own_mix, taken = spread(
        place,
        pieces,
        other_pieces,
        hidden_in,
        other_hidden,
        gain_mix,
        gain_ffn_in,
        routes,
        slots,
    )
    received = lax.all_to_all(
        outgoing, EP, split_axis=0, concat_axis=0, tiled=True
    )
    affinity = jax.nn.sigmoid(jnp.dot(ffn_in, router, preferred_element_type=jnp.float32))
    choose = routes[..., None] == lax.iota(jnp.int32, experts_total)[None, None, :]
    chosen = jnp.sum(jnp.where(choose, affinity[:, None, :], 0.0), axis=-1)
    route_weights = chosen / jnp.sum(chosen, axis=-1, keepdims=True) * routed_scale
    slot_weights = jnp.sum(
        jnp.where(
            routes[:, :, None] == slot_expert[None, None, :], route_weights[:, :, None], 0.0
        ),
        axis=1,
    )
    slot_weights = slot_weights * taken.T.astype(jnp.float32)
    weights_high = slot_weights.astype(jnp.bfloat16)
    weights_low = (slot_weights - weights_high.astype(jnp.float32)).astype(jnp.bfloat16)
    own_ffn = lax.dynamic_slice_in_dim(ffn_in, own_start, seq_count, 0)
    shared = expert_rows(own_ffn, shared_gate, shared_up, shared_down)
    outputs = routed_rows(received, expert_gate[0], expert_up[0], expert_down[0])
    returned = lax.all_to_all(outputs, EP, split_axis=0, concat_axis=0, tiled=True)
    weights = jnp.concatenate([weights_high, weights_low], axis=0)
    kept, given = gathered(place, weights, returned, shared)
    combined = kept + from_other_core(given)
    return (
        own_mix.astype(jnp.float32) + gain_ffn_out.astype(jnp.float32) * normalize(combined)
    ).astype(jnp.bfloat16)


def solution(mesh):
    torus = Mesh(
        mesh.devices.reshape(mesh.shape["grp"], 8, 8, mesh.shape["tp"]),
        ("grp", "ep_0", "ep_1", "tp"),
    )
    in_specs = (
        P(GRP_EP_TP, None),
        P(GRP_EP_TP, None, None),
        P(GRP_EP_TP, None, None),
        P(GRP_EP_TP, None),
        P(GRP_EP_TP, None),
        P(GRP_EP_TP, None, None),
        P(GRP_EP_TP, None, None),
        P(GRP_EP_TP),
        P(),
        P(),
        P(None, EP_TP),
        P(),
        P(),
        P(),
        P(GRP_EP, None),
        P(EP_TP, None, None),
        P(EP_TP, None, None),
        P(EP_TP, None, None),
        P(),
        P(),
        P(),
        P(),
    )
    out_specs = P(GRP_EP_TP, None)

    return jax.shard_map(local, mesh=torus, in_specs=in_specs, out_specs=out_specs, check_vma=False)
```

profile of v0, /device:TPU:513, one launch (start us, length us, event | category | flops | bytes accessed | tf_op | source)
XLA Modules:
  0.0 120.6 jit_solution(5711411289802478415)
XLA Ops:
  0.0 0.0 copy-start
  0.0 0.0 copy-start.4
  0.0 0.9 copy-done.4
  0.9 0.0 copy-start.6
  0.9 0.7 parts.3
  1.6 7.9 %all-to-all-start.1 = ((bf16[8,16,1024]{2,1,0:T(8,128)(2,1)}), bf16[8,16,1024]{2,1,0:T(8,128)(2,1)S(1)}, u32[]{:S(2)}, u32[]{:S(2)}) async-start(bf16[8,16,1024]{2,1,0:T(8,128)(2,1)} %parts.3), calls=%async_computation.1 | async-start | bytes 524288 | tf_op jit(solution)/shard_map/all_to_all | solution.py:91
  9.5 0.0 copy-start.5
  9.5 0.0 copy-start.7
  9.5 0.0 copy-start.8
  9.5 5.5 %attended.1 = bf16[8,16,256]{2,1,0:T(8,128)(2,1)} custom-call(s32[8]{0:T(128)} %lengths_ref.1, bf16[8,16,64]{2,1,0:T(8,128)(2,1)} %nope_ref.1, bf16[8,16,32]{2,1,0:T(8,128)(2,1)} %rope_ref.1, bf16[8,256]{1,0:T(8,128)(2,1)} %latent_ref.1, bf16[8,32]{1,0:T(8,128)(2,1)} %key_ref.1, bf16[1024,256]{1,0:T(8,128)(2,1)} %bitcast.32, ...), custom_call_target="tpu_custom_call" | custom-call | flops 268435456 | bytes 4718592 | tf_op jit(solution)/shard_map/attended/pallas_call | solution.py:227
  15.1 0.0 copy-done
  15.1 1.2 fusion.array_ref
  16.3 0.7 parts.2
  17.0 1.8 %all-to-all-done.1 = bf16[8,16,1024]{2,1,0:T(8,128)(2,1)S(1)} async-done(((bf16[8,16,1024]{2,1,0:T(8,128)(2,1)}), bf16[8,16,1024]{2,1,0:T(8,128)(2,1)S(1)}, u32[]{:S(2)}, u32[]{:S(2)}) %all-to-all-start.1) | async-done | bytes 262176 | tf_op jit(solution)/shard_map/all_to_all | solution.py:91
  18.8 14.5 %all-to-all-start = ((bf16[16,8,1024]{2,1,0:T(8,128)(2,1)}), bf16[16,8,1024]{2,1,0:T(8,128)(2,1)S(1)}, u32[]{:S(2)}, u32[]{:S(2)}) async-start(bf16[16,8,1024]{2,1,0:T(8,128)(2,1)} %parts.2), calls=%async_computation | async-start | bytes 524288 | tf_op jit(solution)/shard_map/all_to_all | solution.py:91
  33.3 6.7 %collective-permute-start.1 = (bf16[128,1024]{1,0:T(8,128)(2,1)S(1)}, bf16[128,1024]{1,0:T(8,128)(2,1)S(1)}, u32[]{:S(2)}, u32[]{:S(2)}) collective-permute-start(bf16[128,1024]{1,0:T(8,128)(2,1)S(1)} %bitcast.25), channel_id=1, source_target_pairs={{0,1},{1,0},{2,3},{3,2},{4,5},{5,4},{6,7},{7,6},{8,9},{9,8},{10,11... | collective-permute-start | bytes 786440 | tf_op jit(solution)/shard_map/ppermute | solution.py:95
  40.0 0.0 copy-done.6
  40.0 0.2 collective-permute-start
  40.2 1.1 collective-permute-done.other_hidden_ref
  41.2 0.4 all-to-all-done.heads_ref
  41.6 0.0 collective-permute-done.1.other_slab_ref
  41.6 0.4 projected.1
  42.1 14.3 %all_to_all.25.own_pieces_ref = bf16[16,8,256]{2,1,0:T(8,128)(2,1)S(1)} all-to-all(bf16[16,8,256]{2,1,0:T(8,128)(2,1)S(1)} %projected.1), channel_id=1, replica_groups={{0,2,16,18,32,34,48,50,64,66,80,82,96,98,112,114},{1,3,17,19,33,35,49,5..., dimensions={0} | all-to-all | bytes 131072 | tf_op jit(solution)/shard_map/all_to_all | solution.py:91
  56.4 5.4 %collective-permute-start.2 = (bf16[16,8,256]{2,1,0:T(8,128)(2,1)S(1)}, bf16[16,8,256]{2,1,0:T(8,128)(2,1)S(1)}, u32[]{:S(2)}, u32[]{:S(2)}) collective-permute-start(bf16[16,8,256]{2,1,0:T(8,128)(2,1)S(1)} %all_to_all.25.own_pieces_ref), channel_id=1, source_target_pairs={{0,1},{1,0},{2,3},{3,2},{4,5},{5,4},{6,7},{7,6},{8,9},{9,8},{10,11... | collective-permute-start | bytes 196616 | tf_op jit(solution)/shard_map/ppermute | solution.py:95
  61.8 0.9 collective-permute-done.2.other_pieces_ref
  62.7 0.0 copy-done.5
  62.7 0.0 copy-done.7
  62.7 0.0 copy-done.8
  62.7 1.3 %spread.1 = (bf16[64,2,2048]{2,1,0:T(2,128)(2,1)}, bf16[16,2048]{1,0:T(8,128)(2,1)S(1)}, bf16[8,2048]{1,0:T(8,128)(2,1)S(1)}, bf16[128,16]{1,0:T(8,128)(2,1)S(1)}) custom-call(s32[1]{0:T(128)} %bitcast.place_ref, bf16[16,8,256]{2,1,0:T(8,128)(2,1)S(1)} %all_to_all.25.own_pieces_ref, bf16[16,8,256]{2,1,0:T(8,128)(2,1)S(1)} %collective-permute-done.2.other_pieces_ref, ...), custom_call_target="tpu_custom_call" | custom-call | tf_op jit(solution)/shard_map/spread/pallas_call | solution.py:345
  64.0 7.1 %all-to-all-start.3 = ((bf16[64,2,2048]{2,1,0:T(2,128)(2,1)}), bf16[64,2,2048]{2,1,0:T(2,128)(2,1)}, u32[]{:S(2)}, u32[]{:S(2)}) async-start(bf16[64,2,2048]{2,1,0:T(2,128)(2,1)} %get-tuple-element.18), calls=%async_computation.3 | async-start | bytes 1048576 | tf_op jit(solution)/shard_map/all_to_all | solution.py:544
  71.1 16.8 %all-to-all-done.3.rows_hbm = bf16[64,2,2048]{2,1,0:T(2,128)(2,1)} async-done(((bf16[64,2,2048]{2,1,0:T(2,128)(2,1)}), bf16[64,2,2048]{2,1,0:T(2,128)(2,1)}, u32[]{:S(2)}, u32[]{:S(2)}) %all-to-all-start.3) | async-done | bytes 524320 | tf_op jit(solution)/shard_map/all_to_all | solution.py:544
  87.9 0.0 copy-start.10
  87.9 3.4 %routed.1 = bf16[64,2,2048]{2,1,0:T(2,128)(2,1)} custom-call(bf16[64,2,2048]{2,1,0:T(2,128)(2,1)} %all-to-all-done.3.rows_hbm, bf16[2048,256]{1,0:T(8,128)(2,1)} %bitcast.29, bf16[2048,256]{1,0:T(8,128)(2,1)} %bitcast.30, bf16[256,2048]{1,0:T(8,128)(2,1)} %bitcast.31), custom_call_target="tpu_custom_call" | custom-call | tf_op jit(solution)/shard_map/routed/pallas_call | solution.py:467
  91.3 0.0 copy-start.9
  91.3 8.0 %all-to-all-start.4 = ((bf16[64,2,2048]{2,1,0:T(2,128)(2,1)}), bf16[64,2,2048]{2,1,0:T(2,128)(2,1)S(1)}, u32[]{:S(2)}, u32[]{:S(2)}) async-start(bf16[64,2,2048]{2,1,0:T(2,128)(2,1)} %routed.1), calls=%async_computation.4 | async-start | bytes 1048576 | tf_op jit(solution)/shard_map/all_to_all | solution.py:563
  99.4 0.1 copy.29
  99.4 0.0 copy-start.1
  99.4 1.2 %copy-done.1 = bf16[2048,256]{1,0:T(8,128)(2,1)S(1)} copy-done((bf16[2048,256]{1,0:T(8,128)(2,1)S(1)}, bf16[2048,256]{1,0:T(8,128)(2,1)}, u32[]{:S(2)}) %copy-start.1) | copy-done | bytes 1048600
  100.7 0.0 copy-start.2
  100.7 1.2 %copy-done.2 = bf16[2048,256]{1,0:T(8,128)(2,1)S(1)} copy-done((bf16[2048,256]{1,0:T(8,128)(2,1)S(1)}, bf16[2048,256]{1,0:T(8,128)(2,1)}, u32[]{:S(2)}) %copy-start.2) | copy-done | bytes 1048600
  101.9 0.0 copy-start.3
  101.9 1.2 %copy-done.3 = bf16[256,2048]{1,0:T(8,128)(2,1)S(1)} copy-done((bf16[256,2048]{1,0:T(8,128)(2,1)S(1)}, bf16[256,2048]{1,0:T(8,128)(2,1)}, u32[]{:S(2)}) %copy-start.3) | copy-done | bytes 1048600
  103.1 0.6 shard_map.208.shared_ref
  103.7 0.0 copy-done.9
  103.7 0.2 fusion.3
  103.9 0.2 select_reduce_fusion
  104.2 0.1 select_reduce_fusion.2
  104.3 10.4 %all-to-all-done.4.returned_ref = bf16[64,2,2048]{2,1,0:T(2,128)(2,1)S(1)} async-done(((bf16[64,2,2048]{2,1,0:T(2,128)(2,1)}), bf16[64,2,2048]{2,1,0:T(2,128)(2,1)S(1)}, u32[]{:S(2)}, u32[]{:S(2)}) %all-to-all-start.4) | async-done | bytes 524320 | tf_op jit(solution)/shard_map/all_to_all | solution.py:563
  114.7 0.2 gathered.1
  114.9 4.0 %collective-permute-start.3 = (f32[8,2048]{1,0:T(8,128)S(1)}, f32[8,2048]{1,0:T(8,128)S(1)}, u32[]{:S(2)}, u32[]{:S(2)}) collective-permute-start(f32[8,2048]{1,0:T(8,128)S(1)} %get-tuple-element.20), channel_id=1, source_target_pairs={{0,1},{1,0},{2,3},{3,2},{4,5},{5,4},{6,7},{7,6},{8,9},{9,8},{10,11... | collective-permute-start | bytes 196616 | tf_op jit(solution)/shard_map/ppermute | solution.py:95
  118.9 0.0 copy-done.10
  118.9 0.9 collective-permute-done.3
  119.8 0.1 multiply_reduce_fusion
  119.9 0.7 add_convert_fusion
  (7 shorter events, 0.0 us)
Async XLA Ops:
  0.0 15.1 %copy-start = (bf16[256,16,128]{2,1,0:T(8,128)(2,1)S(1)}, bf16[256,16,128]{2,1,0:T(8,128)(2,1)}, u32[]{:S(2)}) copy-start(bf16[256,16,128]{2,1,0:T(8,128)(2,1)} %param.31) | copy-start | bytes 3145732
  0.0 0.9 copy-start.4
  0.9 39.1 %copy-start.6 = (bf16[8,2048]{1,0:T(8,128)(2,1)S(1)}, bf16[8,2048]{1,0:T(8,128)(2,1)}, u32[]{:S(2)}) copy-start(bf16[8,2048]{1,0:T(8,128)(2,1)} %own_hidden_ref.1) | copy-start | bytes 98308
  1.6 17.2 %all-to-all-start.1 = ((bf16[8,16,1024]{2,1,0:T(8,128)(2,1)}), bf16[8,16,1024]{2,1,0:T(8,128)(2,1)S(1)}, u32[]{:S(2)}, u32[]{:S(2)}) async-start(bf16[8,16,1024]{2,1,0:T(8,128)(2,1)} %parts.3), calls=%async_computation.1 | async-start | bytes 524288 | tf_op jit(solution)/shard_map/all_to_all | solution.py:91
  9.5 53.2 %copy-start.5 = (s32[16,6]{0,1:T(8,128)S(1)}, s32[16,6]{0,1:T(8,128)}, u32[]{:S(2)}) copy-start(s32[16,6]{0,1:T(8,128)} %param.36) | copy-start | bytes 1156
  9.5 53.2 %copy-start.7 = (bf16[2048]{0:T(1024)(128)(2,1)S(1)}, bf16[2048]{0:T(1024)(128)(2,1)}, u32[]{:S(2)}) copy-start(bf16[2048]{0:T(1024)(128)(2,1)} %gain_mix_ref.1) | copy-start | bytes 12292
  9.5 53.2 %copy-start.8 = (bf16[2048]{0:T(1024)(128)(2,1)S(1)}, bf16[2048]{0:T(1024)(128)(2,1)}, u32[]{:S(2)}) copy-start(bf16[2048]{0:T(1024)(128)(2,1)} %gain_in_ref.1) | copy-start | bytes 12292
  18.8 22.8 %all-to-all-start = ((bf16[16,8,1024]{2,1,0:T(8,128)(2,1)}), bf16[16,8,1024]{2,1,0:T(8,128)(2,1)S(1)}, u32[]{:S(2)}, u32[]{:S(2)}) async-start(bf16[16,8,1024]{2,1,0:T(8,128)(2,1)} %parts.2), calls=%async_computation | async-start | bytes 524288 | tf_op jit(solution)/shard_map/all_to_all | solution.py:91
  33.3 8.3 %collective-permute-start.1 = (bf16[128,1024]{1,0:T(8,128)(2,1)S(1)}, bf16[128,1024]{1,0:T(8,128)(2,1)S(1)}, u32[]{:S(2)}, u32[]{:S(2)}) collective-permute-start(bf16[128,1024]{1,0:T(8,128)(2,1)S(1)} %bitcast.25), channel_id=1, source_target_pairs={{0,1},{1,0},{2,3},{3,2},{4,5},{5,4},{6,7},{7,6},{8,9},{9,8},{10,11... | collective-permute-start | bytes 786440 | tf_op jit(solution)/shard_map/ppermute | solution.py:95
  40.0 1.2 %collective-permute-start = (bf16[8,2048]{1,0:T(8,128)(2,1)S(1)}, bf16[8,2048]{1,0:T(8,128)(2,1)S(1)}, u32[]{:S(2)}, u32[]{:S(2)}) collective-permute-start(bf16[8,2048]{1,0:T(8,128)(2,1)S(1)} %copy-done.6), channel_id=1, source_target_pairs={{0,1},{1,0},{2,3},{3,2},{4,5},{5,4},{6,7},{7,6},{8,9},{9,8},{10,11... | collective-permute-start | bytes 98312 | tf_op jit(solution)/shard_map/ppermute | solution.py:95
  56.4 6.3 %collective-permute-start.2 = (bf16[16,8,256]{2,1,0:T(8,128)(2,1)S(1)}, bf16[16,8,256]{2,1,0:T(8,128)(2,1)S(1)}, u32[]{:S(2)}, u32[]{:S(2)}) collective-permute-start(bf16[16,8,256]{2,1,0:T(8,128)(2,1)S(1)} %all_to_all.25.own_pieces_ref), channel_id=1, source_target_pairs={{0,1},{1,0},{2,3},{3,2},{4,5},{5,4},{6,7},{7,6},{8,9},{9,8},{10,11... | collective-permute-start | bytes 196616 | tf_op jit(solution)/shard_map/ppermute | solution.py:95
  64.0 23.9 %all-to-all-start.3 = ((bf16[64,2,2048]{2,1,0:T(2,128)(2,1)}), bf16[64,2,2048]{2,1,0:T(2,128)(2,1)}, u32[]{:S(2)}, u32[]{:S(2)}) async-start(bf16[64,2,2048]{2,1,0:T(2,128)(2,1)} %get-tuple-element.18), calls=%async_computation.3 | async-start | bytes 1048576 | tf_op jit(solution)/shard_map/all_to_all | solution.py:544
  87.9 31.0 %copy-start.10 = (bf16[2048]{0:T(1024)(128)(2,1)S(1)}, bf16[2048]{0:T(1024)(128)(2,1)}, u32[]{:S(2)}) copy-start(bf16[2048]{0:T(1024)(128)(2,1)} %param.43) | copy-start | bytes 12292
  91.3 12.5 %copy-start.9 = (bf16[2048,128]{1,0:T(8,128)(2,1)S(1)}, bf16[2048,128]{1,0:T(8,128)(2,1)}, u32[]{:S(2)}) copy-start(bf16[2048,128]{1,0:T(8,128)(2,1)} %param.35) | copy-start | bytes 1572868
  91.3 23.4 %all-to-all-start.4 = ((bf16[64,2,2048]{2,1,0:T(2,128)(2,1)}), bf16[64,2,2048]{2,1,0:T(2,128)(2,1)S(1)}, u32[]{:S(2)}, u32[]{:S(2)}) async-start(bf16[64,2,2048]{2,1,0:T(2,128)(2,1)} %routed.1), calls=%async_computation.4 | async-start | bytes 1048576 | tf_op jit(solution)/shard_map/all_to_all | solution.py:563
  99.4 1.3 %copy-start.1 = (bf16[2048,256]{1,0:T(8,128)(2,1)S(1)}, bf16[2048,256]{1,0:T(8,128)(2,1)}, u32[]{:S(2)}) copy-start(bf16[2048,256]{1,0:T(8,128)(2,1)} %gate_ref.1) | copy-start | bytes 3145732
  100.7 1.2 %copy-start.2 = (bf16[2048,256]{1,0:T(8,128)(2,1)S(1)}, bf16[2048,256]{1,0:T(8,128)(2,1)}, u32[]{:S(2)}) copy-start(bf16[2048,256]{1,0:T(8,128)(2,1)} %up_ref.1) | copy-start | bytes 3145732
  101.9 1.2 %copy-start.3 = (bf16[256,2048]{1,0:T(8,128)(2,1)S(1)}, bf16[256,2048]{1,0:T(8,128)(2,1)}, u32[]{:S(2)}) copy-start(bf16[256,2048]{1,0:T(8,128)(2,1)} %down_ref.1) | copy-start | bytes 3145732
  114.9 4.9 %collective-permute-start.3 = (f32[8,2048]{1,0:T(8,128)S(1)}, f32[8,2048]{1,0:T(8,128)S(1)}, u32[]{:S(2)}, u32[]{:S(2)}) collective-permute-start(f32[8,2048]{1,0:T(8,128)S(1)} %get-tuple-element.20), channel_id=1, source_target_pairs={{0,1},{1,0},{2,3},{3,2},{4,5},{5,4},{6,7},{7,6},{8,9},{9,8},{10,11... | collective-permute-start | bytes 196616 | tf_op jit(solution)/shard_map/ppermute | solution.py:95
where the time goes:
time: 121 us
  starting transfers between devices  53.7 us (44%)
  waiting for transfers between devices  32.3 us (27%)
  blocking collectives  14.3 us (12%)
  Pallas kernels  12.9 us (11%)
  local copies, waits for them, and re-layouts  4.73 us (4%)
  matrix products  1.38 us (1%)
    all_to_all x2, starting transfers between devices, exchanged(): lax.all_to_all(blocks, EP_TP, 0, 0, axis_index_groups=groups, tiled=True)  22.3 us
    all_to_all x1, waiting for transfers between devices, local(): lax.all_to_all(outgoing, EP, split_axis=0, concat_axis=0, tiled=True)  16.8 us
    ppermute x4, starting transfers between devices, from_other_core(): return lax.ppermute(array, 'tp', [(0, 1), (1, 0)])  16.2 us
    all_to_all x1, blocking collectives, exchanged(): lax.all_to_all(blocks, EP_TP, 0, 0, axis_index_groups=groups, tiled=True)  14.3 us
    all_to_all x1, waiting for transfers between devices, local(): lax.all_to_all(outputs, EP, split_axis=0, concat_axis=0, tiled=True)  10.4 us
    all_to_all x1, starting transfers between devices, local(): lax.all_to_all(outputs, EP, split_axis=0, concat_axis=0, tiled=True)  8.04 us
    all_to_all x1, starting transfers between devices, local(): lax.all_to_all(outgoing, EP, split_axis=0, concat_axis=0, tiled=True)  7.12 us
    pallas_call x1, Pallas kernels, attended(): pl.pallas_call(attention_kernel, in_specs=[pl.BlockSpec(memory_space=pltp...  5.55 us
  transfers between devices with their start and end apart: 8, of which 7 were waited for; matrix products, arithmetic and copies ran while one was open for 1% of the time, Pallas kernels for 6%

commit v1 on v0

--- a/solution.py
+++ b/solution.py
@@ -476,6 +476,25 @@
     )(rows, gate_w, up_w, down_w)
 
 
+def close_kernel(kept_ref, other_ref, mix_ref, gain_ref, out_ref):
+    combined = kept_ref[...] + other_ref[...]
+    out_ref[...] = (
+        mix_ref[...].astype(jnp.float32)
+        + gain_ref[...].astype(jnp.float32)[None] * normalize(combined)
+    ).astype(jnp.bfloat16)
+
+
+def closed(kept, other, own_mix, gain):
+    return pl.pallas_call(
+        close_kernel,
+        in_specs=[pl.BlockSpec(memory_space=pltpu.VMEM)] * 4,
+        out_specs=pl.BlockSpec(memory_space=pltpu.VMEM),
+        out_shape=jax.ShapeDtypeStruct(kept.shape, jnp.bfloat16),
+        compiler_params=pltpu.CompilerParams(vmem_limit_bytes=4 << 20),
+        name="closed",
+    )(kept, other, own_mix, gain)
+
+
 def local(
     hidden_in,
     query_nope,
@@ -563,10 +582,7 @@
     returned = lax.all_to_all(outputs, EP, split_axis=0, concat_axis=0, tiled=True)
     weights = jnp.concatenate([weights_high, weights_low], axis=0)
     kept, given = gathered(place, weights, returned, shared)
-    combined = kept + from_other_core(given)
-    return (
-        own_mix.astype(jnp.float32) + gain_ffn_out.astype(jnp.float32) * normalize(combined)
-    ).astype(jnp.bfloat16)
+    return closed(kept, from_other_core(given), own_mix, gain_ffn_out)
 
 
 def solution(mesh):

time: 121 us -> 121 us (level)
    unnamed x22 -> x24, local copies, waits for them, and re-layouts: 4.66 us -> 5.46 us
where the time goes in v1:
time: 121 us
  starting transfers between devices  54 us (45%)
  waiting for transfers between devices  31.4 us (26%)
  blocking collectives  14.3 us (12%)
  Pallas kernels  13.5 us (11%)
  local copies, waits for them, and re-layouts  5.53 us (5%)
  matrix products  1.37 us (1%)
    all_to_all x2, starting transfers between devices, exchanged(): lax.all_to_all(blocks, EP_TP, 0, 0, axis_index_groups=groups, tiled=True)  22.3 us
    ppermute x4, starting transfers between devices, from_other_core(): return lax.ppermute(array, 'tp', [(0, 1), (1, 0)])  16.6 us
    all_to_all x1, waiting for transfers between devices, local(): lax.all_to_all(outgoing, EP, split_axis=0, concat_axis=0, tiled=True)  16.2 us
    all_to_all x1, blocking collectives, exchanged(): lax.all_to_all(blocks, EP_TP, 0, 0, axis_index_groups=groups, tiled=True)  14.3 us
    all_to_all x1, waiting for transfers between devices, local(): lax.all_to_all(outputs, EP, split_axis=0, concat_axis=0, tiled=True)  10.1 us
    all_to_all x1, starting transfers between devices, local(): lax.all_to_all(outputs, EP, split_axis=0, concat_axis=0, tiled=True)  8.33 us
    all_to_all x1, starting transfers between devices, local(): lax.all_to_all(outgoing, EP, split_axis=0, concat_axis=0, tiled=True)  6.79 us
    pallas_call x1, Pallas kernels, attended(): pl.pallas_call(attention_kernel, in_specs=[pl.BlockSpec(memory_space=pltp...  5.53 us
  transfers between devices with their start and end apart: 8, of which 7 were waited for; matrix products, arithmetic and copies ran while one was open for 1% of the time, Pallas kernels for 6%

profile of v1, /device:TPU:513, one launch (start us, length us, event | category | flops | bytes accessed | tf_op | source)
XLA Modules:
  0.0 120.7 jit_solution(549468393551638859)
XLA Ops:
  0.0 0.0 copy-start
  0.0 0.0 copy-start.4
  0.0 0.9 copy-done.4
  0.9 0.0 copy-start.6
  0.9 0.7 parts.3
  1.6 7.9 %all-to-all-start.1 = ((bf16[8,16,1024]{2,1,0:T(8,128)(2,1)}), bf16[8,16,1024]{2,1,0:T(8,128)(2,1)S(1)}, u32[]{:S(2)}, u32[]{:S(2)}) async-start(bf16[8,16,1024]{2,1,0:T(8,128)(2,1)} %parts.3), calls=%async_computation.1 | async-start | bytes 524288 | tf_op jit(solution)/shard_map/all_to_all | solution.py:91
  9.5 0.0 copy-start.5
  9.5 0.0 copy-start.7
  9.5 0.0 copy-start.8
  9.5 5.5 %attended.1 = bf16[8,16,256]{2,1,0:T(8,128)(2,1)} custom-call(s32[8]{0:T(128)} %lengths_ref.1, bf16[8,16,64]{2,1,0:T(8,128)(2,1)} %nope_ref.1, bf16[8,16,32]{2,1,0:T(8,128)(2,1)} %rope_ref.1, bf16[8,256]{1,0:T(8,128)(2,1)} %latent_ref.1, bf16[8,32]{1,0:T(8,128)(2,1)} %key_ref.1, bf16[1024,256]{1,0:T(8,128)(2,1)} %bitcast.32, ...), custom_call_target="tpu_custom_call" | custom-call | flops 268435456 | bytes 4718592 | tf_op jit(solution)/shard_map/attended/pallas_call | solution.py:227
  15.1 0.0 copy-done
  15.1 1.2 fusion.array_ref
  16.2 0.7 parts.2
  17.0 1.9 %all-to-all-done.1 = bf16[8,16,1024]{2,1,0:T(8,128)(2,1)S(1)} async-done(((bf16[8,16,1024]{2,1,0:T(8,128)(2,1)}), bf16[8,16,1024]{2,1,0:T(8,128)(2,1)S(1)}, u32[]{:S(2)}, u32[]{:S(2)}) %all-to-all-start.1) | async-done | bytes 262176 | tf_op jit(solution)/shard_map/all_to_all | solution.py:91
  18.8 14.5 %all-to-all-start = ((bf16[16,8,1024]{2,1,0:T(8,128)(2,1)}), bf16[16,8,1024]{2,1,0:T(8,128)(2,1)S(1)}, u32[]{:S(2)}, u32[]{:S(2)}) async-start(bf16[16,8,1024]{2,1,0:T(8,128)(2,1)} %parts.2), calls=%async_computation | async-start | bytes 524288 | tf_op jit(solution)/shard_map/all_to_all | solution.py:91
  33.3 6.7 %collective-permute-start.1 = (bf16[128,1024]{1,0:T(8,128)(2,1)S(1)}, bf16[128,1024]{1,0:T(8,128)(2,1)S(1)}, u32[]{:S(2)}, u32[]{:S(2)}) collective-permute-start(bf16[128,1024]{1,0:T(8,128)(2,1)S(1)} %bitcast.25), channel_id=1, source_target_pairs={{0,1},{1,0},{2,3},{3,2},{4,5},{5,4},{6,7},{7,6},{8,9},{9,8},{10,11... | collective-permute-start | bytes 786440 | tf_op jit(solution)/shard_map/ppermute | solution.py:95
  40.0 0.0 copy-done.6
  40.0 0.2 collective-permute-start
  40.1 1.1 collective-permute-done.other_hidden_ref
  41.2 0.4 all-to-all-done.heads_ref
  41.6 0.0 collective-permute-done.1.other_slab_ref
  41.6 0.4 projected.1
  42.1 14.3 %all_to_all.25.own_pieces_ref = bf16[16,8,256]{2,1,0:T(8,128)(2,1)S(1)} all-to-all(bf16[16,8,256]{2,1,0:T(8,128)(2,1)S(1)} %projected.1), channel_id=1, replica_groups={{0,2,16,18,32,34,48,50,64,66,80,82,96,98,112,114},{1,3,17,19,33,35,49,5..., dimensions={0} | all-to-all | bytes 131072 | tf_op jit(solution)/shard_map/all_to_all | solution.py:91
  56.4 5.4 %collective-permute-start.2 = (bf16[16,8,256]{2,1,0:T(8,128)(2,1)S(1)}, bf16[16,8,256]{2,1,0:T(8,128)(2,1)S(1)}, u32[]{:S(2)}, u32[]{:S(2)}) collective-permute-start(bf16[16,8,256]{2,1,0:T(8,128)(2,1)S(1)} %all_to_all.25.own_pieces_ref), channel_id=1, source_target_pairs={{0,1},{1,0},{2,3},{3,2},{4,5},{5,4},{6,7},{7,6},{8,9},{9,8},{10,11... | collective-permute-start | bytes 196616 | tf_op jit(solution)/shard_map/ppermute | solution.py:95
  61.8 0.9 collective-permute-done.2.other_pieces_ref
  62.7 0.0 copy-done.5
  62.7 0.0 copy-done.7
  62.7 0.0 copy-done.8
  62.7 1.3 %spread.1 = (bf16[64,2,2048]{2,1,0:T(2,128)(2,1)}, bf16[16,2048]{1,0:T(8,128)(2,1)S(1)}, bf16[8,2048]{1,0:T(8,128)(2,1)S(1)}, bf16[128,16]{1,0:T(8,128)(2,1)S(1)}) custom-call(s32[1]{0:T(128)} %bitcast.place_ref, bf16[16,8,256]{2,1,0:T(8,128)(2,1)S(1)} %all_to_all.25.own_pieces_ref, bf16[16,8,256]{2,1,0:T(8,128)(2,1)S(1)} %collective-permute-done.2.other_pieces_ref, ...), custom_call_target="tpu_custom_call" | custom-call | tf_op jit(solution)/shard_map/spread/pallas_call | solution.py:345
  64.0 6.8 %all-to-all-start.3 = ((bf16[64,2,2048]{2,1,0:T(2,128)(2,1)}), bf16[64,2,2048]{2,1,0:T(2,128)(2,1)S(1)}, u32[]{:S(2)}, u32[]{:S(2)}) async-start(bf16[64,2,2048]{2,1,0:T(2,128)(2,1)} %get-tuple-element.17), calls=%async_computation.3 | async-start | bytes 1048576 | tf_op jit(solution)/shard_map/all_to_all | solution.py:563
  70.8 16.2 %all-to-all-done.3.rows_hbm = bf16[64,2,2048]{2,1,0:T(2,128)(2,1)S(1)} async-done(((bf16[64,2,2048]{2,1,0:T(2,128)(2,1)}), bf16[64,2,2048]{2,1,0:T(2,128)(2,1)S(1)}, u32[]{:S(2)}, u32[]{:S(2)}) %all-to-all-start.3) | async-done | bytes 524320 | tf_op jit(solution)/shard_map/all_to_all | solution.py:563
  87.0 0.0 copy-start.10
  87.0 0.8 copy-done.10
  87.8 0.0 copy-start.9
  87.8 3.3 %routed.1 = bf16[64,2,2048]{2,1,0:T(2,128)(2,1)} custom-call(bf16[64,2,2048]{2,1,0:T(2,128)(2,1)} %copy-done.10, bf16[2048,256]{1,0:T(8,128)(2,1)} %bitcast.29, bf16[2048,256]{1,0:T(8,128)(2,1)} %bitcast.30, bf16[256,2048]{1,0:T(8,128)(2,1)} %bitcast.31), custom_call_target="tpu_custom_call" | custom-call | tf_op jit(solution)/shard_map/routed/pallas_call | solution.py:467
  91.1 0.0 copy-start.11
  91.1 8.3 %all-to-all-start.4 = ((bf16[64,2,2048]{2,1,0:T(2,128)(2,1)}), bf16[64,2,2048]{2,1,0:T(2,128)(2,1)S(1)}, u32[]{:S(2)}, u32[]{:S(2)}) async-start(bf16[64,2,2048]{2,1,0:T(2,128)(2,1)} %routed.1), calls=%async_computation.4 | async-start | bytes 1048576 | tf_op jit(solution)/shard_map/all_to_all | solution.py:582
  99.5 0.1 copy.29
  99.6 0.0 copy-start.1
  99.6 1.2 %copy-done.1 = bf16[2048,256]{1,0:T(8,128)(2,1)S(1)} copy-done((bf16[2048,256]{1,0:T(8,128)(2,1)S(1)}, bf16[2048,256]{1,0:T(8,128)(2,1)}, u32[]{:S(2)}) %copy-start.1) | copy-done | bytes 1048600
  100.8 0.0 copy-start.2
  100.8 1.2 %copy-done.2 = bf16[2048,256]{1,0:T(8,128)(2,1)S(1)} copy-done((bf16[2048,256]{1,0:T(8,128)(2,1)S(1)}, bf16[2048,256]{1,0:T(8,128)(2,1)}, u32[]{:S(2)}) %copy-start.2) | copy-done | bytes 1048600
  102.0 0.0 copy-start.3
  102.0 1.2 %copy-done.3 = bf16[256,2048]{1,0:T(8,128)(2,1)S(1)} copy-done((bf16[256,2048]{1,0:T(8,128)(2,1)S(1)}, bf16[256,2048]{1,0:T(8,128)(2,1)}, u32[]{:S(2)}) %copy-start.3) | copy-done | bytes 1048600
  103.3 0.6 shard_map.208.shared_ref
  103.9 0.0 copy-done.11
  103.9 0.2 fusion.3
  104.1 0.2 select_reduce_fusion
  104.3 0.1 select_reduce_fusion.2
  104.4 10.1 %all-to-all-done.4.returned_ref = bf16[64,2,2048]{2,1,0:T(2,128)(2,1)S(1)} async-done(((bf16[64,2,2048]{2,1,0:T(2,128)(2,1)}), bf16[64,2,2048]{2,1,0:T(2,128)(2,1)S(1)}, u32[]{:S(2)}, u32[]{:S(2)}) %all-to-all-start.4) | async-done | bytes 524320 | tf_op jit(solution)/shard_map/all_to_all | solution.py:582
  114.5 0.2 gathered.1
  114.7 4.3 %collective-permute-start.3 = (f32[8,2048]{1,0:T(8,128)S(1)}, f32[8,2048]{1,0:T(8,128)S(1)}, u32[]{:S(2)}, u32[]{:S(2)}) collective-permute-start(f32[8,2048]{1,0:T(8,128)S(1)} %get-tuple-element.19), channel_id=1, source_target_pairs={{0,1},{1,0},{2,3},{3,2},{4,5},{5,4},{6,7},{7,6},{8,9},{9,8},{10,11... | collective-permute-start | bytes 196616 | tf_op jit(solution)/shard_map/ppermute | solution.py:95
  119.0 0.9 collective-permute-done.3.other_ref
  119.9 0.0 copy-done.9
  119.9 0.7 closed.1
  (5 shorter events, 0.0 us)
Async XLA Ops:
  0.0 15.1 %copy-start = (bf16[256,16,128]{2,1,0:T(8,128)(2,1)S(1)}, bf16[256,16,128]{2,1,0:T(8,128)(2,1)}, u32[]{:S(2)}) copy-start(bf16[256,16,128]{2,1,0:T(8,128)(2,1)} %param.31) | copy-start | bytes 3145732
  0.0 0.9 copy-start.4
  0.9 39.1 %copy-start.6 = (bf16[8,2048]{1,0:T(8,128)(2,1)S(1)}, bf16[8,2048]{1,0:T(8,128)(2,1)}, u32[]{:S(2)}) copy-start(bf16[8,2048]{1,0:T(8,128)(2,1)} %own_hidden_ref.1) | copy-start | bytes 98308
  1.6 17.2 %all-to-all-start.1 = ((bf16[8,16,1024]{2,1,0:T(8,128)(2,1)}), bf16[8,16,1024]{2,1,0:T(8,128)(2,1)S(1)}, u32[]{:S(2)}, u32[]{:S(2)}) async-start(bf16[8,16,1024]{2,1,0:T(8,128)(2,1)} %parts.3), calls=%async_computation.1 | async-start | bytes 524288 | tf_op jit(solution)/shard_map/all_to_all | solution.py:91
  9.5 53.2 %copy-start.5 = (s32[16,6]{0,1:T(8,128)S(1)}, s32[16,6]{0,1:T(8,128)}, u32[]{:S(2)}) copy-start(s32[16,6]{0,1:T(8,128)} %param.36) | copy-start | bytes 1156
  9.5 53.2 %copy-start.7 = (bf16[2048]{0:T(1024)(128)(2,1)S(1)}, bf16[2048]{0:T(1024)(128)(2,1)}, u32[]{:S(2)}) copy-start(bf16[2048]{0:T(1024)(128)(2,1)} %gain_mix_ref.1) | copy-start | bytes 12292
  9.5 53.2 %copy-start.8 = (bf16[2048]{0:T(1024)(128)(2,1)S(1)}, bf16[2048]{0:T(1024)(128)(2,1)}, u32[]{:S(2)}) copy-start(bf16[2048]{0:T(1024)(128)(2,1)} %gain_in_ref.1) | copy-start | bytes 12292
  18.8 22.8 %all-to-all-start = ((bf16[16,8,1024]{2,1,0:T(8,128)(2,1)}), bf16[16,8,1024]{2,1,0:T(8,128)(2,1)S(1)}, u32[]{:S(2)}, u32[]{:S(2)}) async-start(bf16[16,8,1024]{2,1,0:T(8,128)(2,1)} %parts.2), calls=%async_computation | async-start | bytes 524288 | tf_op jit(solution)/shard_map/all_to_all | solution.py:91
  33.3 8.3 %collective-permute-start.1 = (bf16[128,1024]{1,0:T(8,128)(2,1)S(1)}, bf16[128,1024]{1,0:T(8,128)(2,1)S(1)}, u32[]{:S(2)}, u32[]{:S(2)}) collective-permute-start(bf16[128,1024]{1,0:T(8,128)(2,1)S(1)} %bitcast.25), channel_id=1, source_target_pairs={{0,1},{1,0},{2,3},{3,2},{4,5},{5,4},{6,7},{7,6},{8,9},{9,8},{10,11... | collective-permute-start | bytes 786440 | tf_op jit(solution)/shard_map/ppermute | solution.py:95
  40.0 1.2 %collective-permute-start = (bf16[8,2048]{1,0:T(8,128)(2,1)S(1)}, bf16[8,2048]{1,0:T(8,128)(2,1)S(1)}, u32[]{:S(2)}, u32[]{:S(2)}) collective-permute-start(bf16[8,2048]{1,0:T(8,128)(2,1)S(1)} %copy-done.6), channel_id=1, source_target_pairs={{0,1},{1,0},{2,3},{3,2},{4,5},{5,4},{6,7},{7,6},{8,9},{9,8},{10,11... | collective-permute-start | bytes 98312 | tf_op jit(solution)/shard_map/ppermute | solution.py:95
  56.4 6.3 %collective-permute-start.2 = (bf16[16,8,256]{2,1,0:T(8,128)(2,1)S(1)}, bf16[16,8,256]{2,1,0:T(8,128)(2,1)S(1)}, u32[]{:S(2)}, u32[]{:S(2)}) collective-permute-start(bf16[16,8,256]{2,1,0:T(8,128)(2,1)S(1)} %all_to_all.25.own_pieces_ref), channel_id=1, source_target_pairs={{0,1},{1,0},{2,3},{3,2},{4,5},{5,4},{6,7},{7,6},{8,9},{9,8},{10,11... | collective-permute-start | bytes 196616 | tf_op jit(solution)/shard_map/ppermute | solution.py:95
  64.0 23.0 %all-to-all-start.3 = ((bf16[64,2,2048]{2,1,0:T(2,128)(2,1)}), bf16[64,2,2048]{2,1,0:T(2,128)(2,1)S(1)}, u32[]{:S(2)}, u32[]{:S(2)}) async-start(bf16[64,2,2048]{2,1,0:T(2,128)(2,1)} %get-tuple-element.17), calls=%async_computation.3 | async-start | bytes 1048576 | tf_op jit(solution)/shard_map/all_to_all | solution.py:563
  87.0 0.8 copy-start.10
  87.8 32.2 %copy-start.9 = (bf16[2048]{0:T(1024)(128)(2,1)S(1)}, bf16[2048]{0:T(1024)(128)(2,1)}, u32[]{:S(2)}) copy-start(bf16[2048]{0:T(1024)(128)(2,1)} %gain_ref.1) | copy-start | bytes 12292
  91.1 12.7 %copy-start.11 = (bf16[2048,128]{1,0:T(8,128)(2,1)S(1)}, bf16[2048,128]{1,0:T(8,128)(2,1)}, u32[]{:S(2)}) copy-start(bf16[2048,128]{1,0:T(8,128)(2,1)} %param.35) | copy-start | bytes 1572868
  91.1 23.4 %all-to-all-start.4 = ((bf16[64,2,2048]{2,1,0:T(2,128)(2,1)}), bf16[64,2,2048]{2,1,0:T(2,128)(2,1)S(1)}, u32[]{:S(2)}, u32[]{:S(2)}) async-start(bf16[64,2,2048]{2,1,0:T(2,128)(2,1)} %routed.1), calls=%async_computation.4 | async-start | bytes 1048576 | tf_op jit(solution)/shard_map/all_to_all | solution.py:582
  99.6 1.3 %copy-start.1 = (bf16[2048,256]{1,0:T(8,128)(2,1)S(1)}, bf16[2048,256]{1,0:T(8,128)(2,1)}, u32[]{:S(2)}) copy-start(bf16[2048,256]{1,0:T(8,128)(2,1)} %gate_ref.1) | copy-start | bytes 3145732
  100.8 1.2 %copy-start.2 = (bf16[2048,256]{1,0:T(8,128)(2,1)S(1)}, bf16[2048,256]{1,0:T(8,128)(2,1)}, u32[]{:S(2)}) copy-start(bf16[2048,256]{1,0:T(8,128)(2,1)} %up_ref.1) | copy-start | bytes 3145732
  102.0 1.2 %copy-start.3 = (bf16[256,2048]{1,0:T(8,128)(2,1)S(1)}, bf16[256,2048]{1,0:T(8,128)(2,1)}, u32[]{:S(2)}) copy-start(bf16[256,2048]{1,0:T(8,128)(2,1)} %down_ref.1) | copy-start | bytes 3145732
  114.7 5.2 %collective-permute-start.3 = (f32[8,2048]{1,0:T(8,128)S(1)}, f32[8,2048]{1,0:T(8,128)S(1)}, u32[]{:S(2)}, u32[]{:S(2)}) collective-permute-start(f32[8,2048]{1,0:T(8,128)S(1)} %get-tuple-element.19), channel_id=1, source_target_pairs={{0,1},{1,0},{2,3},{3,2},{4,5},{5,4},{6,7},{7,6},{8,9},{9,8},{10,11... | collective-permute-start | bytes 196616 | tf_op jit(solution)/shard_map/ppermute | solution.py:95
